TPU v7x, 256 devices: a 4x2x16 block of a 4x16x16 slice. The times are simulated.
256 devices in a mesh: grp: 2 (over y), sp: 32 (over z, core), tp: 4 (over x).
Axes of the slice: x: 4, y: 2, z: 16, core: 2. Of those that a mesh axis runs over, the one named last changes fastest.
The devices are a block of a 4x16x16 slice.
Arguments:
- resid_in: bfloat16 [16384, 2048], P(('grp', 'sp', 'tp')), parts along dimension 0, may hold values from -3 to 3
- queries: bfloat16 [16384, 1024], P(('grp', 'sp'), 'tp'), parts along dimension 0, may hold values from -39 to 39
- keys: bfloat16 [16384, 1024], P(('grp', 'sp'), 'tp'), parts along dimension 0, may hold values from -6 to 6
- values: bfloat16 [16384, 1024], P(('grp', 'sp'), 'tp'), parts along dimension 0, may hold values from -12 to 12
- cum_gate: float32 [16384, 16], P('grp', 'tp'), parts along dimension 0, may hold values from -822 to 0, as said below
- w_out: bfloat16 [1024, 2048], replicated, may hold values from -0.1875 to 0.1875
- norm_gain: float32 [2048], replicated, may hold values from 0.1 to 1.9
- w_gate: bfloat16 [2048, 5632], P('sp', 'tp'), may hold values from -0.125 to 0.125
- w_up: bfloat16 [2048, 5632], P('sp', 'tp'), may hold values from -0.125 to 0.125
- w_down: bfloat16 [5632, 2048], P('tp', 'sp'), may hold values from -0.078125 to 0.078125
Outputs:
- resid_out: bfloat16 [16384, 2048], P(('grp', 'sp', 'tp')), parts along dimension 0
There are 2 independent parts, one for each index of `grp`. A program takes and returns all parts, laid end to end along the dimension named above; an argument that names none is the same for every part. Nothing has to cross between parts.
Inputs may be any that keep to these rules, and one draw needn't show every extreme that they name: `cum_gate`: in every head the values never rise from one position to the next, and the first is at most 0.
All inputs are finite; a program needn't handle non-finite values.
Results may differ from a plain program's by a relative error of at most 0.018.
Values may be sent and summed in bfloat16 or wider, within the bound.
A program may use at most 128 MiB of HBM per device.

v0:
```python
import math

import jax
import jax.numpy as jnp
from jax import lax
from jax.sharding import PartitionSpec as P

HEAD_DIM = 64


def sent_together(arrays, axis, dim, along):
    both = jnp.concatenate(arrays, axis=along)
    filled, at, finished = (lax.all_gather(both, axis, axis=dim, tiled=True), 0, [])
    for a in arrays:
        finished.append(lax.slice_in_dim(filled, at, at + a.shape[along], axis=along))
        at += a.shape[along]
    return tuple(finished)


def laid_out(blocks, dim):
    shape = list(blocks.shape[1:])
    shape[dim] *= blocks.shape[0]
    return jnp.moveaxis(blocks, 0, dim).reshape(shape)


def from_everyone(array, axis):
    length = lax.axis_size(axis)
    return lax.all_to_all(
        jnp.broadcast_to(array[None], (length, *array.shape)), axis, 0, 0, tiled=True
    )


def gathered_copies(array, axis, dim):
    return laid_out(from_everyone(array, axis), dim)


def turned_gather(arrays, axis, dims):
    turned = [jnp.moveaxis(a, dim, 0) for a, dim in zip(arrays, dims)]
    both = jnp.concatenate([t.reshape(len(t), -1) for t in turned], axis=1)
    filled, at, finished = (lax.all_gather(both, axis, axis=0, tiled=True), 0, [])
    for t, dim in zip(turned, dims):
        share = filled[:, at : at + t[0].size].reshape(-1, *t.shape[1:])
        finished.append(jnp.moveaxis(share, 0, dim))
        at += t[0].size
    return tuple(finished)


def in_blocks(array, dim, length):
    shape = array.shape
    blocks = array.reshape(*shape[:dim], length, shape[dim] // length, *shape[dim + 1 :])
    return jnp.moveaxis(blocks, dim, 0)


def sum_at_owner(array, axis, dim):
    length = lax.axis_size(axis)
    blocks = lax.all_to_all(in_blocks(array, dim, length), axis, 0, 0, tiled=True)
    return jnp.sum(blocks.astype(jnp.float32), axis=0)


def on_device(resid_in, queries, keys, values, cum_gate, w_out, norm_gain, w_gate, w_up, w_down):
    tok_rows = queries.shape[0]
    local_heads = queries.shape[1] // HEAD_DIM
    scale = HEAD_DIM ** (-0.5)
    offset = lax.axis_index("sp") * tok_rows
    query_heads = queries.reshape(tok_rows, local_heads, HEAD_DIM)
    own_gate = lax.dynamic_slice_in_dim(cum_gate, offset, tok_rows, 0).T
    query_pos = offset + jnp.arange(tok_rows, dtype=jnp.int32)
    last_pos = offset + tok_rows - 1
    initial = (
        jnp.full((local_heads, tok_rows), -1e30, jnp.float32),
        jnp.zeros((local_heads, tok_rows), jnp.float32),
        jnp.zeros((tok_rows, local_heads, HEAD_DIM), jnp.float32),
    )
    key_piece, value_piece = sent_together((keys, values), "sp", 0, 1)
    length = key_piece.shape[0]
    span = math.gcd(length, 512)

    def block(index, state):
        begin = index * span

        def work(inner):
            maxima, totals, summed = inner
            key_block = lax.dynamic_slice_in_dim(key_piece, index * span, span, 0).reshape(
                span, local_heads, HEAD_DIM
            )
            value_block_rows = lax.dynamic_slice_in_dim(value_piece, index * span, span, 0).reshape(
                span, local_heads, HEAD_DIM
            )
            key_gate = lax.dynamic_slice_in_dim(cum_gate, begin, span, 0).T
            scores = (
                jnp.einsum(
                    "qhd,khd->hqk", query_heads, key_block, preferred_element_type=jnp.float32
                )
                * scale
            )
            scores = scores + own_gate[:, :, None] - key_gate[:, None, :]
            key_pos = begin + jnp.arange(span, dtype=jnp.int32)
            mask = (key_pos[None, :] <= query_pos[:, None])[None]
            scores = jnp.where(mask, scores, -1e30)
            new_max = jnp.maximum(maxima, jnp.max(scores, axis=-1))
            weights = jnp.where(mask, jnp.exp(scores - new_max[:, :, None]), 0.0)
            rescale = jnp.exp(maxima - new_max)
            totals = totals * rescale + jnp.sum(weights, axis=-1)
            product = jnp.einsum(
                "hqk,khd->qhd",
                weights.astype(jnp.bfloat16),
                value_block_rows,
                preferred_element_type=jnp.float32,
            )
            summed = summed * rescale.T[:, :, None] + product
            return (new_max, totals, summed)

        return lax.cond(begin <= last_pos, work, lambda inner: inner, state)

    maxima, totals, summed = lax.fori_loop(0, length // span, block, initial)
    attended = (
        (summed / totals.T[:, :, None])
        .reshape(tok_rows, local_heads * HEAD_DIM)
        .astype(jnp.bfloat16)
    )
    head_rows = lax.all_to_all(attended, "tp", split_axis=0, concat_axis=1, tiled=True)
    mixed = jnp.dot(head_rows, w_out, preferred_element_type=jnp.float32)
    resid = resid_in.astype(jnp.float32) + mixed
    normed = resid * lax.rsqrt(jnp.mean(resid * resid, axis=-1, keepdims=True) + 1e-06)
    normed = (normed * norm_gain).astype(jnp.bfloat16)
    all_rows = gathered_copies(normed, "tp", 0)
    full_gate, full_up, full_down = turned_gather((w_gate, w_up, w_down), "sp", (0, 0, 1))
    gate = jnp.dot(all_rows, full_gate, preferred_element_type=jnp.float32)
    up = jnp.dot(all_rows, full_up, preferred_element_type=jnp.float32)
    hidden = (jax.nn.silu(gate) * up).astype(jnp.bfloat16)
    terms = jnp.dot(hidden, full_down, preferred_element_type=jnp.float32)
    back = sum_at_owner(terms.astype(jnp.bfloat16), "tp", 0)
    return (resid + back).astype(jnp.bfloat16)


def solution(mesh):
    return jax.shard_map(
        on_device,
        mesh=mesh,
        in_specs=(
            P(("grp", "sp", "tp"), None),
            P(("grp", "sp"), "tp"),
            P(("grp", "sp"), "tp"),
            P(("grp", "sp"), "tp"),
            P("grp", "tp"),
            P(),
            P(),
            P("sp", "tp"),
            P("sp", "tp"),
            P("tp", "sp"),
        ),
        out_specs=P(("grp", "sp", "tp"), None),
        check_vma=False,
    )
```

profile of v0, /device:TPU:33, one launch (start us, length us, event | category | flops | bytes accessed | tf_op | source)
XLA Modules:
  0.0 264.1 jit_solution(7843677757114892416)
XLA Ops:
  6.6 1.0 copy.16
  7.6 1.0 copy.17
  8.6 0.7 pad_maximum_fusion.1
  9.3 0.1 all-gather.3.cloned.1.call-update
  9.4 0.1 all-gather.5.cloned.1.call-start
  9.5 2.0 pad_maximum_fusion
  11.4 0.1 all-gather.5.cloned.1.call-update
  11.5 0.1 copy.18
  11.6 0.7 dynamic-slice_bitcast_fusion.1
  12.3 106.1 %all-gather.3.cloned.1.call-done = bf16[8192,512]{0,1:T(8,128)(2,1)} async-done(((bf16[256,512]{0,1:T(8,128)(2,1)}), bf16[8192,512]{0,1:T(8,128)(2,1)}) %all-gather.3.cloned.1.call-update) | async-done | bytes 8388624 | tf_op jit(solution)/shard_map/all_gather | solution.py:13
  118.4 5.9 %fusion.36 = (bf16[8192,256]{0,1:T(8,128)(2,1)}, bf16[8192,256]{0,1:T(8,128)(2,1)}) fusion(bf16[8192,512]{0,1:T(8,128)(2,1)} %all-gather.3.cloned.1.call-done), kind=kLoop, calls=%fused_computation.47 | loop fusion | bytes 16777216 | tf_op jit(solution)/shard_map/slice | solution.py:15
  124.4 4.6 %while.18 = (s32[]{:T(128)}, f32[4,256]{1,0:T(4,128)S(1)}, f32[4,256]{1,0:T(4,128)S(1)}, f32[256,4,64]{0,2,1:T(8,128)S(1)}, s32[]{:T(128)}, /*index=5*/bf16[8192...) while((s32[]{:T(128)}, f32[4,256]{1,0:T(4,128)S(1)}, ...), condition=%wide.region_5.6_spmd.clone, body=%wide.region_0.5_spmd.clone.sunk | while | flops 140250880 | bytes 9146775 | solution.py:115
  124.4 3.7 %conditional.3 = ((f32[4,256]{1,0:T(4,128)S(1)}, f32[4,256]{1,0:T(4,128)S(1)}, f32[256,4,64]{0,2,1:T(8,128)S(1)})) conditional(s32[]{:T(128)} %convert_element_type.56, (f32[4,256]{1,0:T(4,128)S(1)}, f32[4,256]{1,0:T(4,128)S(1)}, f32[256,4,64]{0,2,1:T(8,128)S(1)}) %tuple.47, (s32[]{:T(128)}, s32[]{:T(128)}, s32[]{:T(128)}, ...), branch_computations={%region_1.0_spmd, %region_2.4_spmd} | conditional | flops 140250880 | bytes 9145472 | solution.py:113
  124.5 0.7 dynamic-slice_bitcast_fusion
  125.2 0.1 broadcast_compare_fusion
  125.3 1.1 constant_dynamic-slice_fusion
  126.4 0.7 fusion.35
  127.1 0.5 fusion.4
  127.7 0.4 fusion.3
  129.0 0.2 reshape.69
  129.1 0.2 copy.22
  129.3 8.7 %all_to_all.26 = bf16[4,64,256]{2,1,0:T(8,128)(2,1)S(1)} all-to-all(bf16[4,64,256]{2,1,0:T(8,128)(2,1)S(1)} %copy.22), channel_id=1, replica_groups=mesh['grp'=2,'sp'=32,'tp'=4] {'tp'}, dimensions={0} | all-to-all | bytes 262144 | tf_op jit(solution)/shard_map/all_to_all | solution.py:121
  138.0 3.2 %multiply_reduce_fusion = (f32[64]{0:T(128)S(1)}, f32[64,2048]{1,0:T(8,128)S(1)}) fusion(bf16[64,1024]{1,0:T(8,128)(2,1)S(1)} %bitcast.37, bf16[1024,2048]{1,0:T(8,128)(2,1)} %param.19, bf16[64,2048]{1,0:T(8,128)(2,1)S(1)} %copy-done), kind=kOutput, calls=%fused_computation.40 | convolution fusion | flops 268959680 | bytes 5112064 | tf_op jit(solution)/shard_map/dot_general | solution.py:122
  141.3 0.1 multiply_convert_fusion
  141.4 0.1 broadcast_in_dim.46
  141.5 16.0 %all_to_all.27 = bf16[4,64,2048]{2,1,0:T(8,128)(2,1)S(1)} all-to-all(bf16[4,64,2048]{2,1,0:T(8,128)(2,1)S(1)} %broadcast_in_dim.46), channel_id=1, replica_groups=mesh['grp'=2,'sp'=32,'tp'=4] {'tp'}, dimensions={0} | all-to-all | bytes 2097152 | tf_op jit(solution)/shard_map/all_to_all | solution.py:28
  157.5 66.6 %all-gather.5.cloned.1.call-done = bf16[2048,4224]{1,0:T(8,128)(2,1)} async-done(((bf16[64,4224]{1,0:T(8,128)(2,1)}), bf16[2048,4224]{1,0:T(8,128)(2,1)}) %all-gather.5.cloned.1.call-update) | async-done | bytes 17301520 | tf_op jit(solution)/shard_map/all_gather | solution.py:40
  224.1 5.6 %fusion.15 = f32[256,1408]{1,0:T(8,128)} fusion(bf16[256,2048]{1,0:T(8,128)(2,1)S(1)} %bitcast.33, bf16[2048,4224]{1,0:T(8,128)(2,1)} %all-gather.5.cloned.1.call-done), kind=kOutput, calls=%fused_computation.24 | convolution fusion | flops 1476395008 | bytes 8257536 | tf_op jit(solution)/shard_map/dot_general | solution.py:128
  229.7 8.2 %fusion.23 = bf16[256,2048]{1,0:T(8,128)(2,1)S(1)} fusion(bf16[2048,4224]{1,0:T(8,128)(2,1)} %all-gather.5.cloned.1.call-done, bf16[256,2048]{1,0:T(8,128)(2,1)S(1)} %bitcast.34, f32[256,1408]{1,0:T(8,128)} %fusion.15), kind=kOutput, calls=%fused_computation.28 | convolution fusion | flops 2955476992 | bytes 15073280 | tf_op jit(solution)/shard_map/dot_general | solution.py:131
  237.9 18.4 %all_to_all.28 = bf16[4,64,2048]{2,1,0:T(8,128)(2,1)S(1)} all-to-all(bf16[4,64,2048]{2,1,0:T(8,128)(2,1)S(1)} %bitcast.35), channel_id=1, replica_groups=mesh['grp'=2,'sp'=32,'tp'=4] {'tp'}, dimensions={0} | all-to-all | bytes 2097152 | tf_op jit(solution)/shard_map/all_to_all | solution.py:56
  256.3 0.2 convert_reduce_fusion
  256.5 0.8 add_convert_fusion
  (49 shorter events, 0.4 us)
Async XLA Ops:
  6.5 4.9 %copy-start.1 = (bf16[256,256]{1,0:T(8,128)(2,1)S(1)}, bf16[256,256]{1,0:T(8,128)(2,1)}, u32[]{:S(2)}) copy-start(bf16[256,256]{1,0:T(8,128)(2,1)} %param.15) | copy-start | bytes 393220
  6.5 111.8 %all-gather.3.cloned.1.call-start = ((), (), s32[]{:S(2)}) async-start(), calls=%async_computation.3 | async-start | bytes 8650752 | tf_op jit(solution)/shard_map/all_gather | solution.py:13
  9.4 214.7 %all-gather.5.cloned.1.call-start = ((), (), s32[]{:S(2)}) async-start(), calls=%async_computation.4 | async-start | bytes 17842176 | tf_op jit(solution)/shard_map/all_gather | solution.py:40
  124.4 13.7 %copy-start = (bf16[64,2048]{1,0:T(8,128)(2,1)S(1)}, bf16[64,2048]{1,0:T(8,128)(2,1)}, u32[]{:S(2)}) copy-start(bf16[64,2048]{1,0:T(8,128)(2,1)} %param.14) | copy-start | bytes 786436
  138.0 3.3 %copy-start.2 = (f32[2048]{0:T(1024)S(1)}, f32[2048]{0:T(1024)}, u32[]{:S(2)}) copy-start(f32[2048]{0:T(1024)} %param.20) | copy-start | bytes 24580
Sparse Core Ops, SparseCore 0:
  9.5 108.8 all-gather.2
  120.2 103.8 all-gather.4
where the time goes:
time: 265 us; the launch traced here: 264 us
  waiting for transfers between devices  173 us (65%)
  blocking collectives  43.1 us (16%)
  matrix products  18.3 us (7%)
  between operations  13.6 us (5%)
  local copies, waits for them, and re-layouts  11.1 us (4%)
  other arithmetic  4.31 us (2%)
    all_gather x1, waiting for transfers between devices, sent_together(): lax.all_gather(both, axis, axis=dim, tiled=True)  106 us
    all_gather x1, waiting for transfers between devices, turned_gather(): lax.all_gather(both, axis, axis=0, tiled=True)  66.6 us
    all_to_all x1, blocking collectives, sum_at_owner(): lax.all_to_all(in_blocks(array, dim, length), axis, 0, 0, tiled=True)  18.4 us
    all_to_all x1, blocking collectives, from_everyone(): lax.all_to_all(jnp.broadcast_to(array[None], (length, *array.shape)), axi...  16 us
    all_to_all x1, blocking collectives, on_device(): lax.all_to_all(attended, 'tp', split_axis=0, concat_axis=1, tiled=True)  8.67 us
    dot_general x1, matrix products, on_device(): terms = jnp.dot(hidden, full_down, preferred_element_type=jnp.float32)  8.19 us
    slice x1, local copies, waits for them, and re-layouts, sent_together(): lax.slice_in_dim(filled, at, at + a.shape[along], axis=along)  5.93 us
    dot_general x1, matrix products, on_device(): gate = jnp.dot(all_rows, full_gate, preferred_element_type=jnp.float32)  5.59 us
  transfers between devices with their start and end apart: 2, of which 2 were waited for; matrix products, arithmetic and copies ran while one was open for 6% of the time, Pallas kernels for 0%

commit v1 on v0

v1 whole, which is shorter than its diff:
```python
import functools

import jax
import jax.numpy as jnp
from jax import lax
from jax.experimental import pallas as pl
from jax.experimental.pallas import tpu as pltpu
from jax.sharding import PartitionSpec as P

HEAD_DIM = 64
NEG = -1e30
K, V, G, U, DA, DB = range(6)
UP, DOWN, OWN = range(3)
FAR = {K: UP, V: DOWN, G: UP, U: DOWN, DA: UP, DB: DOWN}
MESH = pl.DeviceIdType.MESH


def kernel(
    nz, ntp,
    resid_in, q_in, k_in, v_in, gate_in, wout_in, gain_in, wg_in, wu_in, wd_in,
    out_ref,
    kbuf, vbuf, wg, wu, wd, qbuf, qm, gate, wout, gain, resid0, resid,
    top, total, acc, att, head_rows, rows, acc_g, acc_u, hidden, terms, psend, precv,
    local_sem, ring_send, ring_recv, pair_send, pair_recv,
    att_send, att_recv, row_send, row_recv, sum_send, sum_recv,
):
    half = nz // 2
    me, t = lax.axis_index("sp"), lax.axis_index("tp")
    z, core = lax.div(me, 2), lax.rem(me, 2)
    partner = me + 1 - 2 * core
    neighbour = (
        2 * lax.rem(z + 1, nz) + core,
        2 * lax.rem(z + nz - 1, nz) + core,
    )
    tok, width = q_in.shape
    heads = width // HEAD_DIM
    own_rows, features = resid_in.shape
    depth, ff = wg_in.shape
    pair = 2 * depth

    def piece(kind, s):
        if kind == K:
            return kbuf.at[s]
        if kind == V:
            return vbuf.at[s]
        if kind == G:
            return wg.at[pl.ds(pl.multiple_of(s * depth, depth), depth)]
        if kind == U:
            return wu.at[pl.ds(pl.multiple_of(s * depth, depth), depth)]
        part = depth // 2
        return wd.at[pl.ds(pl.multiple_of(s * depth + (part if kind == DB else 0), part), part)]

    def owner(way, dist):
        if way == UP:
            return lax.rem(z + nz - dist, nz)
        return lax.rem(z + dist, nz)

    def ring_copy(kind, way, dist):
        ref = piece(kind, 2 * owner(way, dist - 1) + core)
        return pltpu.make_async_remote_copy(
            ref, ref, ring_send.at[kind, way, dist - 1], ring_recv.at[kind, way, dist - 1],
            device_id={"sp": neighbour[way]}, device_id_type=MESH,
        )

    def ring_wait(kind, way, dist):
        ref = piece(kind, 2 * owner(way, dist) + core)
        pltpu.make_async_remote_copy(
            ref, ref, ring_send.at[kind, way, dist - 1], ring_recv.at[kind, way, dist - 1],
            device_id={"sp": neighbour[way]}, device_id_type=MESH,
        ).wait_recv()

    def pair_copy(kind, way, dist, s):
        ref = piece(kind, s)
        return pltpu.make_async_remote_copy(
            ref, ref, pair_send.at[kind, way, dist - 1], pair_recv.at[kind, way, dist - 1],
            device_id={"sp": partner}, device_id_type=MESH,
        )

    def own_start(kind):
        for way in (UP, DOWN):
            ring_copy(kind, way, 1).start()
        pair_copy(kind, OWN, 1, me).start()

    def arrive(kind, dist):
        for way in (UP, DOWN):
            far = FAR[kind] == way

            def take(way=way, far=far):
                ring_wait(kind, way, dist)

                @pl.when(dist < (half if far else half - 1))
                def _():
                    ring_copy(kind, way, dist + 1).start()

                pair_copy(kind, way, dist, 2 * owner(way, dist) + core).start()

            if far:
                take()
            else:
                pl.when(dist < half)(take)

    def pair_wait(kind, way, dist):
        if way == OWN:
            s = partner
        else:
            s = 2 * owner(way, dist) + 1 - core
        pair_copy(kind, way, dist, s).wait_recv()

    def pair_waits(kinds, dist, ways=(UP, DOWN)):
        for kind in kinds:

            @pl.when(dist == 0)
            def _(kind=kind):
                pair_wait(kind, OWN, 1)

            @pl.when(dist == half)
            def _(kind=kind):
                pair_wait(kind, FAR[kind], half)

            @pl.when((dist > 0) & (dist < half))
            def _(kind=kind):
                for way in ways:
                    pair_wait(kind, way, dist)

    def mine(ref):
        return ref.at[pl.ds(pl.multiple_of(me * depth, depth), depth)]

    loads = [
        (k_in, kbuf.at[me]), (v_in, vbuf.at[me]), (q_in, qbuf), (gate_in, gate),
        (wg_in, mine(wg)), (wu_in, mine(wu)), (wd_in, mine(wd)),
        (resid_in, resid0), (wout_in, wout), (gain_in, gain),
    ]
    load = [pltpu.make_async_copy(a, b, local_sem.at[i]) for i, (a, b) in enumerate(loads)]
    for copy in load:
        copy.start()

    barrier = pltpu.get_barrier_semaphore()
    peers = [{"sp": neighbour[UP]}, {"sp": neighbour[DOWN]}, {"sp": partner}]
    across = [lax.rem(t + j, ntp) for j in range(1, ntp)]
    peers += [{"tp": other} for other in across]
    for peer in peers:
        pl.semaphore_signal(barrier, inc=1, device_id=peer, device_id_type=MESH)
    pl.semaphore_wait(barrier, len(peers))

    load[0].wait()
    own_start(K)
    load[1].wait()
    own_start(V)
    load[2].wait()
    load[3].wait()

    turned = (qbuf[...].astype(jnp.float32).T * HEAD_DIM ** (-0.5)).astype(jnp.bfloat16)
    nothing = jnp.zeros((HEAD_DIM, tok), jnp.bfloat16)
    for h in range(heads):
        mine_h = turned[h * HEAD_DIM : (h + 1) * HEAD_DIM]
        qm[h] = jnp.concatenate([mine_h, nothing] if h % 2 == 0 else [nothing, mine_h], axis=0)
    top[...] = jnp.full_like(top, NEG)
    total[...] = jnp.zeros_like(total)
    acc[...] = jnp.zeros_like(acc)

    def attend(s, diagonal):
        key_rows = kbuf[s]
        turned_values = vbuf[s].T
        bias = gate[:, pl.ds(pl.multiple_of(s * tok, tok), tok)]
        bias = jnp.concatenate([bias] * (8 // heads), axis=0).T
        for h in range(heads):
            lanes = slice(h // 2 * 128, h // 2 * 128 + 128)
            scores = jnp.dot(key_rows[:, lanes], qm[h], preferred_element_type=jnp.float32)
            scores = scores - bias[:, h : h + 1]
            if diagonal:
                at = lax.broadcasted_iota(jnp.int32, scores.shape, 0)
                scores = jnp.where(at <= lax.broadcasted_iota(jnp.int32, scores.shape, 1), scores, NEG)
            before = top[h : h + 1, :]
            now = jnp.maximum(before, jnp.max(scores, axis=0, keepdims=True))
            weights = jnp.exp(scores - now)
            rescale = jnp.exp(before - now)
            top[h : h + 1, :] = now
            total[h : h + 1, :] = total[h : h + 1, :] * rescale + jnp.sum(weights, axis=0, keepdims=True)
            part = slice(h * HEAD_DIM, (h + 1) * HEAD_DIM)
            product = jnp.dot(
                turned_values[part], weights.astype(jnp.bfloat16), preferred_element_type=jnp.float32
            )
            acc[part] = acc[part] * rescale + product

    attend(me, True)

    def attention_step(dist, carry):
        @pl.when(dist <= half)
        def _():
            arrive(K, dist)
            arrive(V, dist)

        @pl.when(dist == half - 1)
        def _():
            load[4].wait()
            own_start(G)
            load[5].wait()
            own_start(U)

        last = dist - 1
        pair_waits((K, V), last)

        def job(j, carry):
            way, par = lax.div(j, 2), lax.rem(j, 2)
            zb = lax.rem(z + nz + last * (2 * way - 1), nz)
            s = 2 * zb + core + par * (1 - 2 * core)

            @pl.when(s < me)
            def _():
                attend(s, False)

            return carry

        jobs = 4 - 2 * (lax.div(last, half) + lax.div(half - last, half))
        return lax.fori_loop(0, jobs, job, carry)

    lax.fori_loop(1, half + 2, attention_step, 0)

    sums = jnp.concatenate(
        [
            acc[h * HEAD_DIM : (h + 1) * HEAD_DIM] / total[h : h + 1, :]
            for h in range(heads)
        ],
        axis=0,
    )
    att[...] = sums.T.astype(jnp.bfloat16)

    def rows_of(ref, which):
        return ref.at[pl.ds(pl.multiple_of(which * own_rows, own_rows), own_rows)]

    def att_copy(j):
        return pltpu.make_async_remote_copy(
            rows_of(att, across[j]), head_rows.at[t], att_send.at[j], att_recv.at[j],
            device_id={"tp": across[j]}, device_id_type=MESH,
        )

    def att_wait(j):
        source = lax.rem(t + ntp - 1 - j, ntp)
        pltpu.make_async_remote_copy(
            rows_of(att, across[j]), head_rows.at[source], att_send.at[j], att_recv.at[j],
            device_id={"tp": across[j]}, device_id_type=MESH,
        ).wait_recv()

    arrive(G, 1)
    for j in range(ntp - 1):
        att_copy(j).start()
    head_rows[t] = att[pl.ds(pl.multiple_of(t * own_rows, own_rows), own_rows), :]
    load[7].wait()
    load[8].wait()
    load[9].wait()
    acc_g[...] = jnp.zeros_like(acc_g)
    acc_u[...] = jnp.zeros_like(acc_u)
    for j in range(ntp - 1):
        att_wait(j)
    tile = 256
    squares = jnp.zeros((own_rows, tile), jnp.float32)
    for i in range(features // tile):
        part = slice(i * tile, (i + 1) * tile)
        mixed = jnp.zeros((own_rows, tile), jnp.float32)
        for j in range(ntp):
            mixed += jnp.dot(
                head_rows[j], wout[j * width : (j + 1) * width, part],
                preferred_element_type=jnp.float32,
            )
        mixed = resid0[:, part].astype(jnp.float32) + mixed
        resid[:, part] = mixed
        squares += mixed * mixed
    scale = lax.rsqrt(jnp.sum(squares, axis=1, keepdims=True) / features + 1e-06)
    at_rows = pl.ds(pl.multiple_of(t * own_rows, own_rows), own_rows)
    rows[at_rows, :] = (resid[...] * scale * gain[...]).astype(jnp.bfloat16)

    def row_copy(j, which):
        return pltpu.make_async_remote_copy(
            rows_of(rows, which), rows_of(rows, which), row_send.at[j], row_recv.at[j],
            device_id={"tp": across[j]}, device_id_type=MESH,
        )

    arrive(U, 1)
    for j in range(ntp - 1):
        row_copy(j, t).start()

    def place(index):
        dist = lax.div(index + 1, 2)
        return dist, lax.rem(z + nz + dist * (1 - 2 * lax.rem(index, 2)), nz)

    def pair_ready(kinds, index, dist):
        for kind in kinds:

            @pl.when(dist == 0)
            def _(kind=kind):
                pair_wait(kind, OWN, 1)

            @pl.when(dist == half)
            def _(kind=kind):
                pair_wait(kind, FAR[kind], half)

            for way in (UP, DOWN):

                @pl.when((dist > 0) & (dist < half) & (lax.rem(index, 2) == 1 - way))
                def _(kind=kind, way=way):
                    pair_wait(kind, way, dist)

    first = 4

    def up_step(dist, carry):
        @pl.when(dist <= half)
        def _():
            arrive(G, dist)
            arrive(U, dist)

        @pl.when(dist == half - 1)
        def _():
            load[6].wait()
            own_start(DA)
            own_start(DB)

        @pl.when(dist == first)
        def _():
            for j in range(ntp - 1):
                row_copy(j, lax.rem(t + ntp - 1 - j, ntp)).wait_recv()

        def job(index, carry):
            away, zb = place(index)
            pair_ready((G, U), index, away)
            block = pl.ds(pl.multiple_of(zb * pair, pair), pair)
            left = rows[:, block]
            acc_g[...] += jnp.dot(left, wg[block, :], preferred_element_type=jnp.float32)
            acc_u[...] += jnp.dot(left, wu[block, :], preferred_element_type=jnp.float32)
            return carry

        started = jnp.where(dist < first, 0, 1)
        begin = jnp.where(dist <= first, 0, 2 * dist - 3)
        end = jnp.minimum(2 * dist - 1, nz) * started
        return lax.fori_loop(begin, end, job, carry)

    lax.fori_loop(2, half + 2, up_step, 0)

    def activate(i, carry):
        part = pl.ds(pl.multiple_of(i * 16, 16), 16)
        g = acc_g[part, :]
        hidden[part, :] = (g / (1.0 + jnp.exp(-g)) * acc_u[part, :]).astype(jnp.bfloat16)
        return carry

    lax.fori_loop(0, tok // 16, activate, 0)

    def sum_copy(j, zb):
        return pltpu.make_async_remote_copy(
            psend.at[zb, pl.ds(pl.multiple_of(across[j] * own_rows, own_rows), own_rows)],
            precv.at[j, zb], sum_send.at[j, zb], sum_recv.at[j, zb],
            device_id={"tp": across[j]}, device_id_type=MESH,
        )

    def down_step(dist, carry):
        @pl.when(dist <= half)
        def _():
            arrive(DA, dist)
            arrive(DB, dist)

        def job(index, carry):
            away, zb = place(index)
            pair_ready((DA, DB), index, away)
            block = pl.ds(pl.multiple_of(zb * pair, pair), pair)
            terms[...] = lax.dot_general(
                hidden[...], wd[block, :], (((1,), (1,)), ((), ())),
                preferred_element_type=jnp.float32,
            )
            psend[zb] = terms[...].astype(jnp.bfloat16)
            resid[:, block] += terms[at_rows, :]
            for j in range(ntp - 1):
                sum_copy(j, zb).start()
            return carry

        begin = jnp.maximum(2 * dist - 3, 0)
        lax.fori_loop(begin, jnp.minimum(2 * dist - 1, nz), job, carry)

        def finish(index, carry):
            _, zb = place(index)
            block = pl.ds(pl.multiple_of(zb * pair, pair), pair)
            value = resid[:, block]
            for j in range(ntp - 1):
                sum_copy(j, zb).wait_recv()
                value += precv[j, zb].astype(jnp.float32)
            out_ref[:, block] = value.astype(jnp.bfloat16)
            return carry

        begin = jnp.maximum(2 * dist - 5, 0)
        return lax.fori_loop(begin, jnp.clip(2 * dist - 3, 0, nz), finish, carry)

    lax.fori_loop(1, half + 3, down_step, 0)

    for j in range(ntp - 1):
        att_copy(j).wait_send()
        row_copy(j, t).wait_send()

    def sums_left(zb, carry):
        for j in range(ntp - 1):
            sum_copy(j, zb).wait_send()
        return carry

    lax.fori_loop(0, nz, sums_left, 0)
    for kind in range(6):
        pair_copy(kind, OWN, 1, me).wait_send()
        for way in (UP, DOWN):

            def left(dist, carry, kind=kind, way=way):
                ring_copy(kind, way, dist).wait_send()
                pair_copy(kind, way, dist, 2 * owner(way, dist) + core).wait_send()
                return carry

            lax.fori_loop(1, half + (1 if FAR[kind] == way else 0), left, 0)


def on_device(nsp, ntp, resid_in, queries, keys, values, cum_gate, w_out, norm_gain, w_gate, w_up, w_down):
    nz = nsp // 2
    half = nz // 2
    tok, width = queries.shape
    rows, features = resid_in.shape
    depth, ff = w_gate.shape
    heads = width // HEAD_DIM
    b16, f32 = jnp.bfloat16, jnp.float32
    dma = pltpu.SemaphoreType.DMA
    return pl.pallas_call(
        functools.partial(kernel, nz, ntp),
        out_shape=jax.ShapeDtypeStruct((rows, features), b16),
        in_specs=[pl.BlockSpec(memory_space=pl.ANY)] * 10,
        out_specs=pl.BlockSpec(memory_space=pltpu.VMEM),
        scratch_shapes=[
            pltpu.VMEM((nsp, tok, width), b16),
            pltpu.VMEM((nsp, tok, width), b16),
            pltpu.VMEM((nsp * depth, ff), b16),
            pltpu.VMEM((nsp * depth, ff), b16),
            pltpu.VMEM((nsp * depth, ff), b16),
            pltpu.VMEM((tok, width), b16),
            pltpu.VMEM((heads, 128, tok), b16),
            pltpu.VMEM((heads, nsp * tok), f32),
            pltpu.VMEM(w_out.shape, b16),
            pltpu.VMEM((1, features), f32),
            pltpu.VMEM((rows, features), b16),
            pltpu.VMEM((rows, features), f32),
            pltpu.VMEM((heads, tok), f32),
            pltpu.VMEM((heads, tok), f32),
            pltpu.VMEM((width, tok), f32),
            pltpu.VMEM((tok, width), b16),
            pltpu.VMEM((ntp, rows, width), b16),
            pltpu.VMEM((tok, features), b16),
            pltpu.VMEM((tok, ff), f32),
            pltpu.VMEM((tok, ff), f32),
            pltpu.VMEM((tok, ff), b16),
            pltpu.VMEM((tok, 2 * depth), f32),
            pltpu.VMEM((nz, tok, 2 * depth), b16),
            pltpu.VMEM((ntp - 1, nz, rows, 2 * depth), b16),
            dma((10,)),
            dma((6, 2, half)),
            dma((6, 2, half)),
            dma((6, 3, half)),
            dma((6, 3, half)),
            dma((ntp - 1,)),
            dma((ntp - 1,)),
            dma((ntp - 1,)),
            dma((ntp - 1,)),
            dma((ntp - 1, nz)),
            dma((ntp - 1, nz)),
        ],
        compiler_params=pltpu.CompilerParams(
            collective_id=0, has_side_effects=True, vmem_limit_bytes=60 * 1024 * 1024
        ),
        name="layer",
    )(
        resid_in, queries, keys, values, cum_gate.T, w_out, norm_gain[None, :], w_gate, w_up, w_down.T
    )


def solution(mesh):
    return jax.shard_map(
        functools.partial(on_device, mesh.shape["sp"], mesh.shape["tp"]),
        mesh=mesh,
        in_specs=(
            P(("grp", "sp", "tp"), None),
            P(("grp", "sp"), "tp"),
            P(("grp", "sp"), "tp"),
            P(("grp", "sp"), "tp"),
            P("grp", "tp"),
            P(),
            P(),
            P("sp", "tp"),
            P("sp", "tp"),
            P("tp", "sp"),
        ),
        out_specs=P(("grp", "sp", "tp"), None),
        check_vma=False,
    )
```

time: 265 us -> 185 us (0.70)
  Pallas kernels: 0 us -> 183 us
  waiting for transfers between devices: 173 us -> 0 us
  blocking collectives: 43.1 us -> 0 us
  matrix products: 18.3 us -> 0 us
  between operations: 13.6 us -> 0.01 us
  local copies, waits for them, and re-layouts: 11.1 us -> 1.67 us
  other arithmetic: 4.31 us -> 0 us
    pallas_call x0 -> x1, Pallas kernels: none -> 183 us  [on_device(): pl.pallas_call(functools.partial(kernel, nz, ntp), out_shape=jax.ShapeDty...]
    all_gather x2 -> x0, waiting for transfers between devices: 173 us -> none  [the longest x1 106 us: sent_together(): lax.all_gather(both, axis, axis=dim, tiled=True)]
    all_to_all x3 -> x0, blocking collectives: 43.1 us -> none  [the longest x1 18.4 us: sum_at_owner(): lax.all_to_all(in_blocks(array, dim, length), axis, 0, 0, tiled=True)]
    dot_general x5 -> x0, matrix products: 18.3 us -> none  [the longest x1 8.19 us: on_device(): terms = jnp.dot(hidden, full_down, preferred_element_type=jnp.float32)]
    slice x1 -> x0, local copies, waits for them, and re-layouts: 5.93 us -> none  [sent_together(): lax.slice_in_dim(filled, at, at + a.shape[along], axis=along)]
    concatenate x2 -> x0, other arithmetic: 2.68 us -> none  [the longest x1 1.96 us: turned_gather(): both = jnp.concatenate([t.reshape(len(t), -1) for t in turned], axis=1)]
  transfers between devices with their start and end apart: 2 -> 0, of which waited for: 2 -> 0; matrix products, arithmetic and copies ran while one was open for 6% -> 0% of each run, Pallas kernels for 0% -> 0%
where the time goes in v1:
time: 185 us
  Pallas kernels  183 us (99%)
    pallas_call x1, Pallas kernels, on_device(): pl.pallas_call(functools.partial(kernel, nz, ntp), out_shape=jax.ShapeDty...  183 us

profile of v1, /device:TPU:33, one launch (start us, length us, event | category | flops | bytes accessed | tf_op | source)
XLA Modules:
  0.0 185.1 jit_solution(6730913954608007964)
XLA Ops:
  0.0 183.4 %layer.1 = bf16[64,2048]{1,0:T(8,128)(2,1)} custom-call(bf16[64,2048]{1,0:T(8,128)(2,1)} %resid_in.1, bf16[256,256]{1,0:T(8,128)(2,1)} %q_in.1, bf16[256,256]{1,0:T(8,128)(2,1)} %k_in.1, bf16[256,256]{1,0:T(8,128)(2,1)} %v_in.1, f32[4,8192]{1,0:T(4,128)} %bitcast.4, bf16[1024,2048]{1,0:T(8,128)(2,1)} %wout_in.1, f32[1,2048]{1,0:T(1,128)} %bitcast.5, ...), custom_call_target="tpu_custom_call" | custom-call | tf_op jit(solution)/shard_map/layer/pallas_call | solution.py:422
  183.4 1.7 copy.12

commit v2 on v1

--- a/solution.py
+++ b/solution.py
@@ -9,9 +9,11 @@
 
 HEAD_DIM = 64
 NEG = -1e30
-K, V, G, U, DA, DB = range(6)
+K, V, G, U = range(4)
+D = tuple(range(4, 8))
+KINDS = 8
 UP, DOWN, OWN = range(3)
-FAR = {K: UP, V: DOWN, G: UP, U: DOWN, DA: UP, DB: DOWN}
+FAR = {kind: kind % 2 for kind in range(KINDS)}
 MESH = pl.DeviceIdType.MESH
 
 
@@ -25,6 +27,7 @@
     att_send, att_recv, row_send, row_recv, sum_send, sum_recv,
 ):
     half = nz // 2
+    mid = half // 2
     me, t = lax.axis_index("sp"), lax.axis_index("tp")
     z, core = lax.div(me, 2), lax.rem(me, 2)
     partner = me + 1 - 2 * core
@@ -47,8 +50,8 @@
             return wg.at[pl.ds(pl.multiple_of(s * depth, depth), depth)]
         if kind == U:
             return wu.at[pl.ds(pl.multiple_of(s * depth, depth), depth)]
-        part = depth // 2
-        return wd.at[pl.ds(pl.multiple_of(s * depth + (part if kind == DB else 0), part), part)]
+        part = depth // len(D)
+        return wd.at[pl.ds(pl.multiple_of(s * depth + part * (kind - D[0]), part), part)]
 
     def owner(way, dist):
         if way == UP:
@@ -146,6 +149,8 @@
     own_start(K)
     load[1].wait()
     own_start(V)
+    load[4].wait()
+    own_start(G)
     load[2].wait()
     load[3].wait()
 
@@ -190,12 +195,21 @@
             arrive(K, dist)
             arrive(V, dist)
 
-        @pl.when(dist == half - 1)
-        def _():
-            load[4].wait()
-            own_start(G)
+        @pl.when(dist == 1)
+        def _():
             load[5].wait()
             own_start(U)
+
+        @pl.when((dist > 1) & (dist <= half))
+        def _():
+            pl.when(lax.rem(dist, 2) == 0)(lambda: arrive(G, lax.div(dist, 2)))
+            pl.when(lax.rem(dist, 2) == 1)(lambda: arrive(U, lax.div(dist, 2)))
+
+        @pl.when(dist == half)
+        def _():
+            load[6].wait()
+            for kind in D:
+                own_start(kind)
 
         last = dist - 1
         pair_waits((K, V), last)
@@ -241,9 +255,9 @@
             device_id={"tp": across[j]}, device_id_type=MESH,
         ).wait_recv()
 
-    arrive(G, 1)
     for j in range(ntp - 1):
         att_copy(j).start()
+    arrive(U, mid)
     head_rows[t] = att[pl.ds(pl.multiple_of(t * own_rows, own_rows), own_rows), :]
     load[7].wait()
     load[8].wait()
@@ -275,9 +289,14 @@
             device_id={"tp": across[j]}, device_id_type=MESH,
         )
 
-    arrive(U, 1)
+    def forward_down(dist):
+        for kind in D:
+            arrive(kind, dist)
+
+    arrive(G, mid + 1)
     for j in range(ntp - 1):
         row_copy(j, t).start()
+    forward_down(1)
 
     def place(index):
         dist = lax.div(index + 1, 2)
@@ -300,19 +319,20 @@
                 def _(kind=kind, way=way):
                     pair_wait(kind, way, dist)
 
-    first = 4
+    first = mid + 2
 
     def up_step(dist, carry):
         @pl.when(dist <= half)
         def _():
-            arrive(G, dist)
             arrive(U, dist)
 
-        @pl.when(dist == half - 1)
-        def _():
-            load[6].wait()
-            own_start(DA)
-            own_start(DB)
+        @pl.when(dist < half)
+        def _():
+            arrive(G, dist + 1)
+
+        @pl.when(dist <= half)
+        def _():
+            forward_down(dist - mid + 1)
 
         @pl.when(dist == first)
         def _():
@@ -333,7 +353,7 @@
         end = jnp.minimum(2 * dist - 1, nz) * started
         return lax.fori_loop(begin, end, job, carry)
 
-    lax.fori_loop(2, half + 2, up_step, 0)
+    lax.fori_loop(mid + 1, half + 2, up_step, 0)
 
     def activate(i, carry):
         part = pl.ds(pl.multiple_of(i * 16, 16), 16)
@@ -350,15 +370,16 @@
             device_id={"tp": across[j]}, device_id_type=MESH,
         )
 
+    start = half - mid + 2
+
     def down_step(dist, carry):
         @pl.when(dist <= half)
         def _():
-            arrive(DA, dist)
-            arrive(DB, dist)
+            forward_down(dist)
 
         def job(index, carry):
             away, zb = place(index)
-            pair_ready((DA, DB), index, away)
+            pair_ready(D, index, away)
             block = pl.ds(pl.multiple_of(zb * pair, pair), pair)
             terms[...] = lax.dot_general(
                 hidden[...], wd[block, :], (((1,), (1,)), ((), ())),
@@ -370,7 +391,7 @@
                 sum_copy(j, zb).start()
             return carry
 
-        begin = jnp.maximum(2 * dist - 3, 0)
+        begin = jnp.where(dist == start, 0, 2 * dist - 3)
         lax.fori_loop(begin, jnp.minimum(2 * dist - 1, nz), job, carry)
 
         def finish(index, carry):
@@ -383,10 +404,10 @@
             out_ref[:, block] = value.astype(jnp.bfloat16)
             return carry
 
-        begin = jnp.maximum(2 * dist - 5, 0)
-        return lax.fori_loop(begin, jnp.clip(2 * dist - 3, 0, nz), finish, carry)
-
-    lax.fori_loop(1, half + 3, down_step, 0)
+        begin = jnp.where(dist <= start + 1, 0, 2 * dist - 5)
+        return lax.fori_loop(begin, jnp.where(dist == start, 0, jnp.minimum(2 * dist - 3, nz)), finish, carry)
+
+    lax.fori_loop(start, half + 3, down_step, 0)
 
     for j in range(ntp - 1):
         att_copy(j).wait_send()
@@ -398,7 +419,7 @@
         return carry
 
     lax.fori_loop(0, nz, sums_left, 0)
-    for kind in range(6):
+    for kind in range(KINDS):
         pair_copy(kind, OWN, 1, me).wait_send()
         for way in (UP, DOWN):
 
@@ -450,10 +471,10 @@
             pltpu.VMEM((nz, tok, 2 * depth), b16),
             pltpu.VMEM((ntp - 1, nz, rows, 2 * depth), b16),
             dma((10,)),
-            dma((6, 2, half)),
-            dma((6, 2, half)),
-            dma((6, 3, half)),
-            dma((6, 3, half)),
+            dma((KINDS, 2, half)),
+            dma((KINDS, 2, half)),
+            dma((KINDS, 3, half)),
+            dma((KINDS, 3, half)),
             dma((ntp - 1,)),
             dma((ntp - 1,)),
             dma((ntp - 1,)),

time: 185 us -> 177 us (0.957)
  Pallas kernels: 183 us -> 175 us
    pallas_call x1, Pallas kernels: 183 us -> 175 us  [on_device(): pl.pallas_call(functools.partial(kernel, nz, ntp), out_shape=jax.ShapeDty...]
where the time goes in v2:
time: 177 us; the launch traced here: 176 us
  Pallas kernels  175 us (99%)
    pallas_call x1, Pallas kernels, on_device(): pl.pallas_call(functools.partial(kernel, nz, ntp), out_shape=jax.ShapeDty...  175 us

profile of v2, /device:TPU:33, one launch (start us, length us, event | category | flops | bytes accessed | tf_op | source)
XLA Modules:
  0.0 176.4 jit_solution(8101773267522057781)
XLA Ops:
  0.0 174.7 %layer.1 = bf16[64,2048]{1,0:T(8,128)(2,1)} custom-call(bf16[64,2048]{1,0:T(8,128)(2,1)} %resid_in.1, bf16[256,256]{1,0:T(8,128)(2,1)} %q_in.1, bf16[256,256]{1,0:T(8,128)(2,1)} %k_in.1, bf16[256,256]{1,0:T(8,128)(2,1)} %v_in.1, f32[4,8192]{1,0:T(4,128)} %bitcast.4, bf16[1024,2048]{1,0:T(8,128)(2,1)} %wout_in.1, f32[1,2048]{1,0:T(1,128)} %bitcast.5, ...), custom_call_target="tpu_custom_call" | custom-call | tf_op jit(solution)/shard_map/layer/pallas_call | solution.py:443
  174.7 1.7 copy.12

commit v3 on v2

--- a/solution.py
+++ b/solution.py
@@ -79,37 +79,55 @@
             device_id={"sp": partner}, device_id_type=MESH,
         )
 
+    def goes(kind, way, dist, s):
+        if kind not in (K, V):
+            return True
+        if way == UP:
+            return s + dist < nz
+        return s < (half if FAR[kind] == way else half - 1)
+
+    def used(kind, way, dist):
+        return True if kind not in (K, V) else owner(way, dist) < z
+
+    def guard(condition, run):
+        if condition is True:
+            run()
+        else:
+            pl.when(condition)(run)
+
     def own_start(kind):
         for way in (UP, DOWN):
-            ring_copy(kind, way, 1).start()
+            guard(goes(kind, way, 1, z), lambda way=way: ring_copy(kind, way, 1).start())
         pair_copy(kind, OWN, 1, me).start()
 
     def arrive(kind, dist):
         for way in (UP, DOWN):
             far = FAR[kind] == way
-
-            def take(way=way, far=far):
+            s = owner(way, dist)
+
+            def take(way=way, far=far, s=s):
                 ring_wait(kind, way, dist)
 
                 @pl.when(dist < (half if far else half - 1))
                 def _():
-                    ring_copy(kind, way, dist + 1).start()
-
-                pair_copy(kind, way, dist, 2 * owner(way, dist) + core).start()
-
+                    guard(goes(kind, way, dist + 1, s), lambda: ring_copy(kind, way, dist + 1).start())
+
+                guard(used(kind, way, dist), lambda: pair_copy(kind, way, dist, 2 * s + core).start())
+
+            comes = goes(kind, way, dist, s)
             if far:
-                take()
+                guard(comes, take)
             else:
-                pl.when(dist < half)(take)
+                pl.when(dist < half if comes is True else (dist < half) & comes)(take)
 
     def pair_wait(kind, way, dist):
         if way == OWN:
-            s = partner
+            pair_copy(kind, OWN, 1, partner).wait_recv()
         else:
             s = 2 * owner(way, dist) + 1 - core
-        pair_copy(kind, way, dist, s).wait_recv()
-
-    def pair_waits(kinds, dist, ways=(UP, DOWN)):
+            guard(used(kind, way, dist), lambda: pair_copy(kind, way, dist, s).wait_recv())
+
+    def pair_waits(kinds, dist):
         for kind in kinds:
 
             @pl.when(dist == 0)
@@ -122,7 +140,7 @@
 
             @pl.when((dist > 0) & (dist < half))
             def _(kind=kind):
-                for way in ways:
+                for way in (UP, DOWN):
                     pair_wait(kind, way, dist)
 
     def mine(ref):
@@ -151,6 +169,8 @@
     own_start(V)
     load[4].wait()
     own_start(G)
+    load[5].wait()
+    own_start(U)
     load[2].wait()
     load[3].wait()
 
@@ -194,11 +214,6 @@
         def _():
             arrive(K, dist)
             arrive(V, dist)
-
-        @pl.when(dist == 1)
-        def _():
-            load[5].wait()
-            own_start(U)
 
         @pl.when((dist > 1) & (dist <= half))
         def _():
@@ -296,7 +311,6 @@
     arrive(G, mid + 1)
     for j in range(ntp - 1):
         row_copy(j, t).start()
-    forward_down(1)
 
     def place(index):
         dist = lax.div(index + 1, 2)
@@ -330,9 +344,9 @@
         def _():
             arrive(G, dist + 1)
 
-        @pl.when(dist <= half)
-        def _():
-            forward_down(dist - mid + 1)
+        @pl.when((dist > mid + 1) & (dist <= half))
+        def _():
+            forward_down(dist - mid - 1)
 
         @pl.when(dist == first)
         def _():
@@ -370,7 +384,7 @@
             device_id={"tp": across[j]}, device_id_type=MESH,
         )
 
-    start = half - mid + 2
+    start = half - mid
 
     def down_step(dist, carry):
         @pl.when(dist <= half)
@@ -424,8 +438,14 @@
         for way in (UP, DOWN):
 
             def left(dist, carry, kind=kind, way=way):
-                ring_copy(kind, way, dist).wait_send()
-                pair_copy(kind, way, dist, 2 * owner(way, dist) + core).wait_send()
+                guard(
+                    goes(kind, way, dist, owner(way, dist - 1)),
+                    lambda: ring_copy(kind, way, dist).wait_send(),
+                )
+                guard(
+                    used(kind, way, dist),
+                    lambda: pair_copy(kind, way, dist, 2 * owner(way, dist) + core).wait_send(),
+                )
                 return carry
 
             lax.fori_loop(1, half + (1 if FAR[kind] == way else 0), left, 0)

time: 177 us -> 176 us (level)
  no operation moved by 1% of the time
where the time goes in v3:
time: 176 us
  Pallas kernels  174 us (99%)
    pallas_call x1, Pallas kernels, on_device(): pl.pallas_call(functools.partial(kernel, nz, ntp), out_shape=jax.ShapeDty...  174 us

profile of v3, /device:TPU:33, one launch (start us, length us, event | category | flops | bytes accessed | tf_op | source)
XLA Modules:
  0.0 175.6 jit_solution(6850919384280865111)
XLA Ops:
  0.0 173.9 %layer.1 = bf16[64,2048]{1,0:T(8,128)(2,1)} custom-call(bf16[64,2048]{1,0:T(8,128)(2,1)} %resid_in.1, bf16[256,256]{1,0:T(8,128)(2,1)} %q_in.1, bf16[256,256]{1,0:T(8,128)(2,1)} %k_in.1, bf16[256,256]{1,0:T(8,128)(2,1)} %v_in.1, f32[4,8192]{1,0:T(4,128)} %bitcast.4, bf16[1024,2048]{1,0:T(8,128)(2,1)} %wout_in.1, f32[1,2048]{1,0:T(1,128)} %bitcast.5, ...), custom_call_target="tpu_custom_call" | custom-call | tf_op jit(solution)/shard_map/layer/pallas_call | solution.py:463
  173.9 1.7 copy.12

commit v4 on v3

--- a/solution.py
+++ b/solution.py
@@ -333,39 +333,49 @@
                 def _(kind=kind, way=way):
                     pair_wait(kind, way, dist)
 
-    first = mid + 2
+    first, turns = mid + 2, 6
+
+    def up_done(dist):
+        return jnp.clip(jnp.minimum(turns * (dist - first + 1), 2 * dist - 1), 0, nz)
 
     def up_step(dist, carry):
-        @pl.when(dist <= half)
-        def _():
-            arrive(U, dist)
-
-        @pl.when(dist < half)
-        def _():
-            arrive(G, dist + 1)
-
-        @pl.when((dist > mid + 1) & (dist <= half))
-        def _():
-            forward_down(dist - mid - 1)
-
-        @pl.when(dist == first)
-        def _():
-            for j in range(ntp - 1):
-                row_copy(j, lax.rem(t + ntp - 1 - j, ntp)).wait_recv()
-
-        def job(index, carry):
-            away, zb = place(index)
-            pair_ready((G, U), index, away)
-            block = pl.ds(pl.multiple_of(zb * pair, pair), pair)
-            left = rows[:, block]
-            acc_g[...] += jnp.dot(left, wg[block, :], preferred_element_type=jnp.float32)
-            acc_u[...] += jnp.dot(left, wu[block, :], preferred_element_type=jnp.float32)
+        def turn(j, carry):
+            @pl.when((j == 0) & (dist <= half))
+            def _():
+                arrive(U, dist)
+
+            @pl.when((j == 2) & (dist < half))
+            def _():
+                arrive(G, dist + 1)
+
+            @pl.when((j == 4) & (dist > mid + 1) & (dist <= half))
+            def _():
+                forward_down(dist - mid - 1)
+
+            @pl.when((j == 4) & (dist == half - 1))
+            def _():
+                for i in range(ntp - 1):
+                    att_copy(i).wait_send()
+
+            @pl.when((j == 0) & (dist == first))
+            def _():
+                for i in range(ntp - 1):
+                    row_copy(i, lax.rem(t + ntp - 1 - i, ntp)).wait_recv()
+
+            index = up_done(dist - 1) + j
+
+            @pl.when(index < up_done(dist))
+            def _():
+                away, zb = place(index)
+                pair_ready((G, U), index, away)
+                block = pl.ds(pl.multiple_of(zb * pair, pair), pair)
+                left = rows[:, block]
+                acc_g[...] += jnp.dot(left, wg[block, :], preferred_element_type=jnp.float32)
+                acc_u[...] += jnp.dot(left, wu[block, :], preferred_element_type=jnp.float32)
+
             return carry
 
-        started = jnp.where(dist < first, 0, 1)
-        begin = jnp.where(dist <= first, 0, 2 * dist - 3)
-        end = jnp.minimum(2 * dist - 1, nz) * started
-        return lax.fori_loop(begin, end, job, carry)
+        return lax.fori_loop(0, turns, turn, carry)
 
     lax.fori_loop(mid + 1, half + 2, up_step, 0)
 
@@ -386,27 +396,67 @@
 
     start = half - mid
 
+    def down_done(dist):
+        return jnp.clip(jnp.minimum(len(D) * (dist - start + 1), 2 * dist - 1), 0, nz)
+
+    def sent(kinds, begin, end):
+        for kind in kinds:
+            for way in (UP, DOWN):
+
+                def left(dist, carry, kind=kind, way=way):
+                    guard(
+                        goes(kind, way, dist, owner(way, dist - 1)),
+                        lambda: ring_copy(kind, way, dist).wait_send(),
+                    )
+                    guard(
+                        used(kind, way, dist),
+                        lambda: pair_copy(kind, way, dist, 2 * owner(way, dist) + core).wait_send(),
+                    )
+                    return carry
+
+                reach = half if FAR[kind] == way else half - 1
+                lax.fori_loop(begin, min(end, reach + 1), left, 0)
+
     def down_step(dist, carry):
-        @pl.when(dist <= half)
+        def turn(j, carry):
+            for i, kind in enumerate(D):
+
+                @pl.when((j == i) & (dist <= half))
+                def _(kind=kind):
+                    arrive(kind, dist)
+
+            index = down_done(dist - 1) + j
+
+            @pl.when(index < down_done(dist))
+            def _():
+                away, zb = place(index)
+                pair_ready(D, index, away)
+                block = pl.ds(pl.multiple_of(zb * pair, pair), pair)
+                terms[...] = lax.dot_general(
+                    hidden[...], wd[block, :], (((1,), (1,)), ((), ())),
+                    preferred_element_type=jnp.float32,
+                )
+                psend[zb] = terms[...].astype(jnp.bfloat16)
+                resid[:, block] += terms[at_rows, :]
+                for i in range(ntp - 1):
+                    sum_copy(i, zb).start()
+
+            return carry
+
+        lax.fori_loop(0, len(D), turn, 0)
+
+        @pl.when(dist == start)
         def _():
-            forward_down(dist)
-
-        def job(index, carry):
-            away, zb = place(index)
-            pair_ready(D, index, away)
-            block = pl.ds(pl.multiple_of(zb * pair, pair), pair)
-            terms[...] = lax.dot_general(
-                hidden[...], wd[block, :], (((1,), (1,)), ((), ())),
-                preferred_element_type=jnp.float32,
-            )
-            psend[zb] = terms[...].astype(jnp.bfloat16)
-            resid[:, block] += terms[at_rows, :]
             for j in range(ntp - 1):
-                sum_copy(j, zb).start()
-            return carry
-
-        begin = jnp.where(dist == start, 0, 2 * dist - 3)
-        lax.fori_loop(begin, jnp.minimum(2 * dist - 1, nz), job, carry)
+                row_copy(j, t).wait_send()
+            for kind in range(KINDS):
+                pair_copy(kind, OWN, 1, me).wait_send()
+            sent((K, V), 1, half + 1)
+
+        pl.when(dist == start + 1)(lambda: sent((G,), 1, half + 1))
+        pl.when(dist == start + 2)(lambda: sent((U,), 1, half + 1))
+        pl.when(dist == half - 1)(lambda: sent(D, 1, half - 1))
+        pl.when(dist == half)(lambda: sent(D, half - 1, half))
 
         def finish(index, carry):
             _, zb = place(index)
@@ -414,41 +464,17 @@
             value = resid[:, block]
             for j in range(ntp - 1):
                 sum_copy(j, zb).wait_recv()
+                sum_copy(j, zb).wait_send()
                 value += precv[j, zb].astype(jnp.float32)
             out_ref[:, block] = value.astype(jnp.bfloat16)
             return carry
 
-        begin = jnp.where(dist <= start + 1, 0, 2 * dist - 5)
-        return lax.fori_loop(begin, jnp.where(dist == start, 0, jnp.minimum(2 * dist - 3, nz)), finish, carry)
+        return lax.fori_loop(down_done(dist - 2), down_done(dist - 1), finish, carry)
 
     lax.fori_loop(start, half + 3, down_step, 0)
 
-    for j in range(ntp - 1):
-        att_copy(j).wait_send()
-        row_copy(j, t).wait_send()
-
-    def sums_left(zb, carry):
-        for j in range(ntp - 1):
-            sum_copy(j, zb).wait_send()
-        return carry
-
-    lax.fori_loop(0, nz, sums_left, 0)
-    for kind in range(KINDS):
-        pair_copy(kind, OWN, 1, me).wait_send()
-        for way in (UP, DOWN):
-
-            def left(dist, carry, kind=kind, way=way):
-                guard(
-                    goes(kind, way, dist, owner(way, dist - 1)),
-                    lambda: ring_copy(kind, way, dist).wait_send(),
-                )
-                guard(
-                    used(kind, way, dist),
-                    lambda: pair_copy(kind, way, dist, 2 * owner(way, dist) + core).wait_send(),
-                )
-                return carry
-
-            lax.fori_loop(1, half + (1 if FAR[kind] == way else 0), left, 0)
+    for kind in D:
+        sent((kind,), half, half + 1)
 
 
 def on_device(nsp, ntp, resid_in, queries, keys, values, cum_gate, w_out, norm_gain, w_gate, w_up, w_down):
@@ -462,7 +488,7 @@
     dma = pltpu.SemaphoreType.DMA
     return pl.pallas_call(
         functools.partial(kernel, nz, ntp),
-        out_shape=jax.ShapeDtypeStruct((rows, features), b16),
+        out_shape=pltpu.VMEM((rows, features), b16),
         in_specs=[pl.BlockSpec(memory_space=pl.ANY)] * 10,
         out_specs=pl.BlockSpec(memory_space=pltpu.VMEM),
         scratch_shapes=[

time: 176 us -> 171 us (0.972)
  Pallas kernels: 174 us -> 171 us
    pallas_call x1, Pallas kernels: 174 us -> 171 us  [on_device(): pl.pallas_call(functools.partial(kernel, nz, ntp), out_shape=pltpu.VMEM((...]
where the time goes in v4:
time: 171 us
  Pallas kernels  171 us (100%)
    pallas_call x1, Pallas kernels, on_device(): pl.pallas_call(functools.partial(kernel, nz, ntp), out_shape=pltpu.VMEM((...  171 us

profile of v4, /device:TPU:33, one launch (start us, length us, event | category | flops | bytes accessed | tf_op | source)
XLA Modules:
  0.0 171.3 jit_solution(10723440907900897560)
XLA Ops:
  0.0 170.5 %layer.1 = bf16[64,2048]{1,0:T(8,128)(2,1)S(1)} custom-call(bf16[64,2048]{1,0:T(8,128)(2,1)} %resid_in.1, bf16[256,256]{1,0:T(8,128)(2,1)} %q_in.1, bf16[256,256]{1,0:T(8,128)(2,1)} %k_in.1, bf16[256,256]{1,0:T(8,128)(2,1)} %v_in.1, f32[4,8192]{1,0:T(4,128)} %bitcast.4, bf16[1024,2048]{1,0:T(8,128)(2,1)} %wout_in.1, f32[1,2048]{1,0:T(1,128)} %bitcast.5, ...), custom_call_target="tpu_custom_call" | custom-call | tf_op jit(solution)/shard_map/layer/pallas_call | solution.py:489
  170.6 0.7 copy.12

commit v5 on v4

--- a/solution.py
+++ b/solution.py
@@ -146,6 +146,12 @@
     def mine(ref):
         return ref.at[pl.ds(pl.multiple_of(me * depth, depth), depth)]
 
+    barrier = pltpu.get_barrier_semaphore()
+    peers = [{"sp": neighbour[UP]}, {"sp": neighbour[DOWN]}, {"sp": partner}]
+    across = [lax.rem(t + j, ntp) for j in range(1, ntp)]
+    peers += [{"tp": other} for other in across]
+    for peer in peers:
+        pl.semaphore_signal(barrier, inc=1, device_id=peer, device_id_type=MESH)
     loads = [
         (k_in, kbuf.at[me]), (v_in, vbuf.at[me]), (q_in, qbuf), (gate_in, gate),
         (wg_in, mine(wg)), (wu_in, mine(wu)), (wd_in, mine(wd)),
@@ -154,13 +160,6 @@
     load = [pltpu.make_async_copy(a, b, local_sem.at[i]) for i, (a, b) in enumerate(loads)]
     for copy in load:
         copy.start()
-
-    barrier = pltpu.get_barrier_semaphore()
-    peers = [{"sp": neighbour[UP]}, {"sp": neighbour[DOWN]}, {"sp": partner}]
-    across = [lax.rem(t + j, ntp) for j in range(1, ntp)]
-    peers += [{"tp": other} for other in across]
-    for peer in peers:
-        pl.semaphore_signal(barrier, inc=1, device_id=peer, device_id_type=MESH)
     pl.semaphore_wait(barrier, len(peers))
 
     load[0].wait()
@@ -438,7 +437,7 @@
                 )
                 psend[zb] = terms[...].astype(jnp.bfloat16)
                 resid[:, block] += terms[at_rows, :]
-                for i in range(ntp - 1):
+                for i in sorted(range(ntp - 1), key=lambda i: -min(i + 1, ntp - 1 - i)):
                     sum_copy(i, zb).start()
 
             return carry

time: 171 us -> 171 us (level)
  no operation moved by 1% of the time
where the time goes in v5:
time: 171 us
  Pallas kernels  170 us (99%)
    pallas_call x1, Pallas kernels, on_device(): pl.pallas_call(functools.partial(kernel, nz, ntp), out_shape=pltpu.VMEM((...  170 us

profile of v5, /device:TPU:33, one launch (start us, length us, event | category | flops | bytes accessed | tf_op | source)
XLA Modules:
  0.0 171.1 jit_solution(6748250998531357200)
XLA Ops:
  0.0 170.3 %layer.1 = bf16[64,2048]{1,0:T(8,128)(2,1)S(1)} custom-call(bf16[64,2048]{1,0:T(8,128)(2,1)} %resid_in.1, bf16[256,256]{1,0:T(8,128)(2,1)} %q_in.1, bf16[256,256]{1,0:T(8,128)(2,1)} %k_in.1, bf16[256,256]{1,0:T(8,128)(2,1)} %v_in.1, f32[4,8192]{1,0:T(4,128)} %bitcast.4, bf16[1024,2048]{1,0:T(8,128)(2,1)} %wout_in.1, f32[1,2048]{1,0:T(1,128)} %bitcast.5, ...), custom_call_target="tpu_custom_call" | custom-call | tf_op jit(solution)/shard_map/layer/pallas_call | solution.py:488
  170.4 0.7 copy.12

commit v6 on v5

--- a/solution.py
+++ b/solution.py
@@ -112,13 +112,22 @@
                 def _():
                     guard(goes(kind, way, dist + 1, s), lambda: ring_copy(kind, way, dist + 1).start())
 
-                guard(used(kind, way, dist), lambda: pair_copy(kind, way, dist, 2 * s + core).start())
-
             comes = goes(kind, way, dist, s)
             if far:
                 guard(comes, take)
             else:
                 pl.when(dist < half if comes is True else (dist < half) & comes)(take)
+
+        for way in (UP, DOWN):
+
+            def hand(way=way):
+                pair_copy(kind, way, dist, 2 * owner(way, dist) + core).start()
+
+            wanted = used(kind, way, dist)
+            if FAR[kind] == way:
+                guard(wanted, hand)
+            else:
+                pl.when(dist < half if wanted is True else (dist < half) & wanted)(hand)
 
     def pair_wait(kind, way, dist):
         if way == OWN:

time: 171 us -> 171 us (level)
  no operation moved by 1% of the time
where the time goes in v6:
time: 171 us
  Pallas kernels  170 us (99%)
    pallas_call x1, Pallas kernels, on_device(): pl.pallas_call(functools.partial(kernel, nz, ntp), out_shape=pltpu.VMEM((...  170 us

profile of v6, /device:TPU:33, one launch (start us, length us, event | category | flops | bytes accessed | tf_op | source)
XLA Modules:
  0.0 171.1 jit_solution(16399873272378452443)
XLA Ops:
  0.0 170.4 %layer.1 = bf16[64,2048]{1,0:T(8,128)(2,1)S(1)} custom-call(bf16[64,2048]{1,0:T(8,128)(2,1)} %resid_in.1, bf16[256,256]{1,0:T(8,128)(2,1)} %q_in.1, bf16[256,256]{1,0:T(8,128)(2,1)} %k_in.1, bf16[256,256]{1,0:T(8,128)(2,1)} %v_in.1, f32[4,8192]{1,0:T(4,128)} %bitcast.4, bf16[1024,2048]{1,0:T(8,128)(2,1)} %wout_in.1, f32[1,2048]{1,0:T(1,128)} %bitcast.5, ...), custom_call_target="tpu_custom_call" | custom-call | tf_op jit(solution)/shard_map/layer/pallas_call | solution.py:497
  170.4 0.7 copy.12
